TPU v7x, 128 devices: a whole 4x4x4 slice. The times are simulated.
128 devices in a mesh: ep: 128 (over z, y, x, core).
Axes of the slice: x: 4, y: 4, z: 4, core: 2. Of those that a mesh axis runs over, the one named last changes fastest.
Arguments:
- tokens: bfloat16 [1536, 2048], P('ep'), may hold values from -6 to 6
- cache_latent: bfloat16 [1536, 1024, 512], P('ep'), may hold values from -180 to 180
- cache_rope: bfloat16 [1536, 1024, 64], P('ep'), may hold values from -6 to 6
- cache_lengths: int32 [1536], P('ep'), may hold values from 1 to 1024, as said below
- expert_ids: int32 [1536, 6], P('ep'), may hold values from 0 to 63, as said below
- route_weight: float32 [1536, 6], P('ep'), may hold values from 1 to 2
- attn_gain: float32 [2048], replicated, may hold values from 0.1 to 1.9
- q_gain: float32 [512], replicated, may hold values from 0.1 to 1.9
- kv_gain: float32 [512], replicated, may hold values from 0.1 to 1.9
- moe_gain: float32 [2048], replicated, may hold values from 0.1 to 1.9
- w_qdown: bfloat16 [2048, 512], replicated, may hold values from -0.125 to 0.125
- w_kvdown: bfloat16 [2048, 512], replicated, may hold values from -0.125 to 0.125
- w_krope: bfloat16 [2048, 64], replicated, may hold values from -0.125 to 0.125
- w_qup: bfloat16 [512, 1536], replicated, may hold values from -0.25 to 0.25
- w_kup: bfloat16 [512, 1024], replicated, may hold values from -0.5 to 0.5
- w_vup: bfloat16 [512, 1024], replicated, may hold values from -0.25 to 0.25
- w_out: bfloat16 [1024, 2048], replicated, may hold values from -0.1875 to 0.1875
- expert_gate: bfloat16 [128, 2048, 256], P('ep'), may hold values from -0.125 to 0.125
- expert_up: bfloat16 [128, 2048, 256], P('ep'), may hold values from -0.125 to 0.125
- expert_down: bfloat16 [128, 256, 2048], P('ep'), may hold values from -0.25 to 0.25
Outputs:
- mixed: float32 [1536, 2048], P('ep')
- new_latent: bfloat16 [1536, 512], P('ep')
- new_rope_key: bfloat16 [1536, 64], P('ep')
Inputs may be any that keep to these rules, and one draw needn't show every extreme that they name: `cache_lengths`: some sequence holds 1024 positions. `expert_ids`: each row names 6 different experts of one group g, numbered g * 16 to g * 16 + 15; among the rows of one device no expert is named more than 3 times, and some expert exactly 3 times.
All inputs are finite; a program needn't handle non-finite values.
Results may differ from a plain program's by a relative error of at most 0.03.
Values may be sent and summed in bfloat16 or wider, within the bound.
A program may use at most 128 MiB of HBM per device.

v0:
```python
import jax
import jax.numpy as jnp
from jax import lax
from jax.sharding import PartitionSpec as P

HEADS = 8
KV_RANK = 512
NOPE_DIM = 128
ROPE_DIM = 64
VALUE_DIM = 128
GROUP_SIZE = 16
TOP_K = 6
BLOCK_POS = 512
SEQ_DEV = 12


EPS = 1e-06
THETA = 10000.0


def partner(value, axis, bit):
    mask = 2**bit
    pairs = [(source, source ^ mask) for source in range(lax.axis_size(axis))]
    return lax.ppermute(value, axis, pairs)


def norm_gain(values, gain_vec):
    values = values.astype(jnp.float32)
    return values * lax.rsqrt(jnp.mean(values * values, axis=-1, keepdims=True) + EPS) * gain_vec


def rotary_angles(lengths):
    half_width = ROPE_DIM // 2
    inverse = THETA ** (-jnp.arange(half_width, dtype=jnp.float32) / half_width)
    return lengths.astype(jnp.float32)[:, None] * inverse[None, :]


def rotate(values, angles):
    half_width = values.shape[-1] // 2
    first_half = values[..., :half_width]
    second = values[..., half_width:]
    cosine = jnp.cos(angles)
    sine_part = jnp.sin(angles)
    return jnp.concatenate(
        [first_half * cosine - second * sine_part, second * cosine + first_half * sine_part],
        axis=-1,
    )


def attend(
    tokens,
    cache_latent,
    cache_rope,
    cache_lengths,
    attn_gain,
    q_gain,
    kv_gain,
    w_qdown,
    w_kvdown,
    w_krope,
    w_qup,
    w_kup,
    w_vup,
    w_out,
):
    row_count = tokens.shape[0]
    score_scale = (NOPE_DIM + ROPE_DIM) ** (-0.5)
    normed = norm_gain(tokens, attn_gain).astype(jnp.bfloat16)
    q_low = norm_gain(jnp.dot(normed, w_qdown, preferred_element_type=jnp.float32), q_gain).astype(
        jnp.bfloat16
    )
    query_all = jnp.dot(q_low, w_qup, preferred_element_type=jnp.float32).reshape(
        row_count, HEADS, NOPE_DIM + ROPE_DIM
    )
    angles = rotary_angles(cache_lengths)
    q_nope = query_all[:, :, :NOPE_DIM].astype(jnp.bfloat16)
    q_rope = rotate(query_all[:, :, NOPE_DIM:], angles[:, None, :]).astype(jnp.bfloat16)
    new_latent = norm_gain(
        jnp.dot(normed, w_kvdown, preferred_element_type=jnp.float32), kv_gain
    ).astype(jnp.bfloat16)
    new_rope_key = rotate(
        jnp.dot(normed, w_krope, preferred_element_type=jnp.float32), angles
    ).astype(jnp.bfloat16)
    q_latent = jnp.einsum(
        "thn,chn->thc",
        q_nope,
        w_kup.reshape(KV_RANK, HEADS, NOPE_DIM),
        preferred_element_type=jnp.float32,
    ).astype(jnp.bfloat16)
    own_score = (
        jnp.einsum("thc,tc->th", q_latent, new_latent, preferred_element_type=jnp.float32)
        + jnp.einsum("thr,tr->th", q_rope, new_rope_key, preferred_element_type=jnp.float32)
    ) * score_scale
    run_sum = jnp.broadcast_to(
        new_latent.astype(jnp.float32)[:, None, :], (row_count, HEADS, KV_RANK)
    )
    run_total = jnp.ones((row_count, HEADS), jnp.float32)
    block_total = (jnp.max(cache_lengths) + BLOCK_POS - 1) // BLOCK_POS

    def block_step(block_index, carry):
        run_peak, run_total, run_sum = carry
        block_start = block_index * BLOCK_POS
        latent_block = lax.dynamic_slice_in_dim(cache_latent, block_start, BLOCK_POS, 1)
        rope_block = lax.dynamic_slice_in_dim(cache_rope, block_start, BLOCK_POS, 1)
        scores = (
            jnp.einsum("thc,tpc->thp", q_latent, latent_block, preferred_element_type=jnp.float32)
            + jnp.einsum("thr,tpr->thp", q_rope, rope_block, preferred_element_type=jnp.float32)
        ) * score_scale
        valid_mask = (block_start + jnp.arange(BLOCK_POS, dtype=jnp.int32))[
            None, None, :
        ] < cache_lengths[:, None, None]
        scores = jnp.where(valid_mask, scores, -jnp.inf)
        new_peak = jnp.maximum(run_peak, jnp.max(scores, axis=2))
        shrink = jnp.exp(run_peak - new_peak)
        block_probs = jnp.exp(scores - new_peak[:, :, None])
        run_total = run_total * shrink + jnp.sum(block_probs, axis=2)
        run_sum = run_sum * shrink[:, :, None] + jnp.einsum(
            "thp,tpc->thc",
            block_probs.astype(jnp.bfloat16),
            latent_block,
            preferred_element_type=jnp.float32,
        )
        return (new_peak, run_total, run_sum)

    run_peak, run_total, run_sum = lax.fori_loop(
        0, block_total, block_step, (own_score, run_total, run_sum)
    )
    o_latent = (run_sum / run_total[:, :, None]).astype(jnp.bfloat16)
    heads_out = (
        jnp.einsum(
            "thc,chv->thv",
            o_latent,
            w_vup.reshape(KV_RANK, HEADS, VALUE_DIM),
            preferred_element_type=jnp.float32,
        )
        .astype(jnp.bfloat16)
        .reshape(row_count, HEADS * VALUE_DIM)
    )
    mixed_attn = (
        tokens.astype(jnp.float32) + jnp.dot(heads_out, w_out, preferred_element_type=jnp.float32)
    ).astype(jnp.bfloat16)
    return (mixed_attn, new_latent, new_rope_key)


def capacity_of(half_count):
    group_count = half_count // 2 // GROUP_SIZE
    group_most = min(SEQ_DEV, max(3, 2 * ((SEQ_DEV + group_count - 1) // group_count)))
    return (TOP_K * group_most + GROUP_SIZE - 1) // GROUP_SIZE


def mix_experts(moe_in, expert_ids, route_weight, expert_gate, expert_up, expert_down):
    row_count, model_width = moe_in.shape
    top_count = expert_ids.shape[1]
    half_count = lax.axis_size("ep")
    slot_count = capacity_of(half_count)
    per_core = (slot_count + 1) // 2
    gate_half = expert_gate[0]
    up_half = expert_up[0]
    down_half = expert_down[0]
    flat_ids = expert_ids.reshape(-1)
    one_hot = (flat_ids[:, None] == jnp.arange(half_count // 2, dtype=jnp.int32)[None, :]).astype(
        jnp.int32
    )
    earlier = jnp.cumsum(one_hot, axis=0) - one_hot
    slot_rank = jnp.sum(earlier * one_hot, axis=1)
    owner_ids = jnp.arange(half_count, dtype=jnp.int32) // 2
    parity_ids = jnp.arange(half_count, dtype=jnp.int32) % 2
    wanted_rank = (
        2 * jnp.arange(per_core, dtype=jnp.int32)[None, None, :] + parity_ids[None, :, None]
    )
    placed = (flat_ids[:, None, None] == owner_ids[None, :, None]) & (
        slot_rank[:, None, None] == wanted_rank
    )
    placed = placed.reshape(row_count * top_count, half_count * per_core).astype(jnp.float32)
    chosen = jnp.max(placed.reshape(row_count, top_count, half_count * per_core), axis=1).astype(
        jnp.bfloat16
    )
    outgoing = jnp.einsum("sx,sd->xd", chosen, moe_in, preferred_element_type=jnp.float32).astype(
        jnp.bfloat16
    )
    own_rows = lax.all_to_all(
        outgoing.reshape(half_count, per_core, model_width),
        "ep",
        split_axis=0,
        concat_axis=0,
        tiled=True,
    )
    sibling = partner(own_rows, "ep", 0)
    slot_rows = jnp.concatenate([own_rows, sibling], axis=1)
    flat_rows = slot_rows.reshape(-1, model_width)
    hidden = (
        jax.nn.silu(jnp.dot(flat_rows, gate_half, preferred_element_type=jnp.float32))
        * jnp.dot(flat_rows, up_half, preferred_element_type=jnp.float32)
    ).astype(jnp.bfloat16)
    outputs = (
        jnp.dot(hidden, down_half, preferred_element_type=jnp.float32)
        .astype(jnp.bfloat16)
        .reshape(slot_rows.shape)
    )
    from_sibling = partner(outputs[:, per_core:], "ep", 0)
    pair_sum = outputs[:, :per_core].astype(jnp.float32) + from_sibling.astype(jnp.float32)
    returned = lax.all_to_all(pair_sum, "ep", split_axis=0, concat_axis=0, tiled=True)
    per_route = jnp.dot(
        placed,
        returned.reshape(half_count * per_core, model_width),
        preferred_element_type=jnp.float32,
    )
    per_route = per_route.reshape(row_count, top_count, model_width)
    return jnp.sum(route_weight[:, :, None] * per_route, axis=1)


def shards(
    tokens,
    cache_latent,
    cache_rope,
    cache_lengths,
    expert_ids,
    route_weight,
    attn_gain,
    q_gain,
    kv_gain,
    moe_gain,
    w_qdown,
    w_kvdown,
    w_krope,
    w_qup,
    w_kup,
    w_vup,
    w_out,
    expert_gate,
    expert_up,
    expert_down,
):
    mixer_weights = (
        attn_gain,
        q_gain,
        kv_gain,
        w_qdown,
        w_kvdown,
        w_krope,
        w_qup,
        w_kup,
        w_vup,
        w_out,
    )
    mixed_attn, new_latent, new_rope_key = attend(
        tokens, cache_latent, cache_rope, cache_lengths, *mixer_weights
    )
    moe_in = norm_gain(mixed_attn, moe_gain).astype(jnp.bfloat16)
    moe_out = mix_experts(moe_in, expert_ids, route_weight, expert_gate, expert_up, expert_down)
    mixed = mixed_attn.astype(jnp.float32) + moe_out
    return (mixed, new_latent, new_rope_key)


def solution(mesh):
    placed = (
        P("ep", None),
        P("ep", None, None),
        P("ep", None, None),
        P("ep"),
        P("ep", None),
        P("ep", None),
        P(),
        P(),
        P(),
        P(),
        P(),
        P(),
        P(),
        P(),
        P(),
        P(),
        P(),
        P("ep", None, None),
        P("ep", None, None),
        P("ep", None, None),
    )
    return jax.shard_map(
        shards,
        mesh=mesh,
        in_specs=placed,
        out_specs=(P("ep", None), P("ep", None), P("ep", None)),
        check_vma=False,
    )
```

profile of v0, /device:TPU:0, one launch (start us, length us, event | category | flops | bytes accessed | tf_op | source)
XLA Modules:
  0.0 129.9 jit_solution(14234093944366156090)
XLA Ops:
  0.7 1.5 %fusion.65 = (s32[]{:T(128)}, f32[12]{0:T(128)S(1)}) fusion(s32[12]{0:T(128)} %param.25), kind=kLoop, calls=%fused_computation.104 | loop fusion | flops 23 | bytes 100 | tf_op jit(solution)/shard_map/reduce_max | solution.py:98
  2.8 0.5 multiply_power_fusion
  3.3 1.0 fusion.40
  4.3 1.4 %multiply_reduce_fusion.1 = (f32[12]{0:T(128)S(1)}, f32[12,512]{1,0:T(8,128)S(1)}) fusion(bf16[2048,512]{1,0:T(8,128)(2,1)S(1)} %copy-done, bf16[12,2048]{1,0:T(8,128)(2,1)} %param.22, f32[2048]{0:T(1024)} %param.28, f32[12]{0:T(128)S(1)} %add_rsqrt_fusion.3), kind=kOutput, calls=%fused_computation.70 | convolution fusion | flops 25276404 | bytes 2179168 | tf_op jit(solution)/shard_map/dot_general | solution.py:79
  5.9 0.6 and_select_fusion.1
  6.5 2.3 %multiply_reduce_fusion.2 = (f32[12]{0:T(128)S(1)}, f32[12,512]{1,0:T(8,128)S(1)}) fusion(bf16[2048,512]{1,0:T(8,128)(2,1)} %param.32, bf16[12,2048]{1,0:T(8,128)(2,1)S(1)} %copy-done.4, f32[2048]{0:T(1024)S(1)} %copy-done.7, f32[12]{0:T(128)S(1)} %add_rsqrt_fusion.3), kind=kOutput, calls=%fused_computation.72 | convolution fusion | flops 25276404 | bytes 2179168 | tf_op jit(solution)/shard_map/dot_general | solution.py:69
  8.8 0.4 fusion.51
  9.2 0.1 reshape.305
  9.3 1.2 fusion.58
  10.5 0.4 fusion.24
  10.9 0.1 copy.50
  11.0 0.8 subtract_convert_fusion.1
  11.7 0.1 subtract_convert_fusion
  11.8 0.1 pad_maximum_fusion.1
  11.9 0.1 fusion.81
  12.0 0.1 fusion.55
  12.1 0.1 fusion.49
  12.3 18.1 %while.14 = (s32[]{:T(128)}, f32[12,8]{1,0:T(8,128)S(1)}, f32[12,8]{1,0:T(8,128)S(1)}, f32[12,8,512]{2,1,0:T(8,128)S(1)}, s32[]{:T(128)}, /*index=5*/s32[12]{0:T...) while((s32[]{:T(128)}, f32[12,8]{1,0:T(8,128)S(1)}, ...), condition=%wide.region_7.8_spmd, body=%wide.region_4.7_spmd.sunk | while | flops 107453120 | bytes 21184784 | solution.py:125
  12.4 4.6 %fusion.98 = f32[12,512,8]{1,2,0:T(8,128)S(1)} fusion(bf16[12,8,512]{2,1,0:T(8,128)(2,1)S(1)} %get-tuple-element.242, bf16[12,1024,512]{2,1,0:T(8,128)(2,1)} %get-tuple-element.241, s32[]{:T(128)S(6)} %select_n.46), kind=kOutput, calls=%fused_computation.2.clone.1 | convolution fusion | flops 50331648 | bytes 6586372 | tf_op jit(solution)/shard_map/while/body/thc,tpc->thp/dot_general | solution.py:106
  17.1 0.3 fusion.99
  17.4 0.2 fusion.100
  17.6 3.7 %fusion.101 = f32[12,8,512]{2,1,0:T(8,128)S(1)} fusion(bf16[12,1024,512]{2,1,0:T(8,128)(2,1)} %get-tuple-element.241, s32[]{:T(128)S(6)} %select_n.46, f32[12,8,512]{2,1,0:T(8,128)S(1)} %get-tuple-element.224, f32[12,8,512]{2,1,0:T(8,128)S(1)} %get-tuple-element.204, f32[12,8]{1,0:T(8,128)S(1)} %get-tuple-element.206, f32[12,8]{1,0:T(8,128)S(1)} %max.4), kind=kOutput, calls=%fused_computation.6.clone.1 | convolution fusion | flops 50528256 | bytes 6882052 | tf_op jit(solution)/shard_map/while/body/thp,tpc->thc/dot_general | solution.py:117
  21.4 4.6 %fusion.98 = f32[12,512,8]{1,2,0:T(8,128)S(1)} fusion(bf16[12,8,512]{2,1,0:T(8,128)(2,1)S(1)} %get-tuple-element.242, bf16[12,1024,512]{2,1,0:T(8,128)(2,1)} %get-tuple-element.241, s32[]{:T(128)S(6)} %select_n.46), kind=kOutput, calls=%fused_computation.2.clone.1 | convolution fusion | flops 50331648 | bytes 6586372 | tf_op jit(solution)/shard_map/while/body/thc,tpc->thp/dot_general | solution.py:106
  26.0 0.1 broadcast_compare_fusion.3
  26.1 0.3 fusion.99
  26.4 0.2 fusion.100
  26.6 3.7 %fusion.101 = f32[12,8,512]{2,1,0:T(8,128)S(1)} fusion(bf16[12,1024,512]{2,1,0:T(8,128)(2,1)} %get-tuple-element.241, s32[]{:T(128)S(6)} %select_n.46, f32[12,8,512]{2,1,0:T(8,128)S(1)} %get-tuple-element.224, f32[12,8,512]{2,1,0:T(8,128)S(1)} %get-tuple-element.204, f32[12,8]{1,0:T(8,128)S(1)} %get-tuple-element.206, f32[12,8]{1,0:T(8,128)S(1)} %max.4), kind=kOutput, calls=%fused_computation.6.clone.1 | convolution fusion | flops 50528256 | bytes 6882052 | tf_op jit(solution)/shard_map/while/body/thp,tpc->thc/dot_general | solution.py:117
  30.4 0.1 divide_convert_fusion
  30.5 1.5 %fusion.25 = bf16[12,8,128]{2,0,1:T(8,128)(2,1)S(1)} fusion(bf16[12,8,512]{2,1,0:T(8,128)(2,1)S(1)} %divide_convert_fusion, bf16[512,1024]{1,0:T(8,128)(2,1)} %param.37), kind=kOutput, calls=%fused_computation.35 | convolution fusion | flops 12595200 | bytes 1171456 | tf_op jit(solution)/shard_map/thc,chv->thv/dot_general | solution.py:130
  32.1 3.0 %multiply_reduce_fusion = (f32[12]{0:T(128)S(1)}, f32[12,2048]{1,0:T(8,128)S(1)}) fusion(bf16[12,1024]{1,0:T(8,128)(2,1)S(1)} %bitcast.70, bf16[1024,2048]{1,0:T(8,128)(2,1)} %param.38, bf16[12,2048]{1,0:T(8,128)(2,1)S(1)} %copy-done.4), kind=kOutput, calls=%fused_computation.56 | convolution fusion | flops 50479092 | bytes 4366384 | tf_op jit(solution)/shard_map/dot_general | solution.py:140
  35.1 0.1 copy.55
  35.2 0.1 eq.66
  35.3 0.1 fusion.47
  35.4 0.1 reduce_window_sum.11
  35.5 0.2 select_reduce_fusion
  35.7 0.1 eq.76
  35.7 0.1 broadcast_compare_fusion.1
  35.9 1.0 and.62
  36.9 0.1 add.143
  37.1 0.2 add.145
  37.3 1.7 %convert_reduce_fusion = bf16[12,256]{0,1:T(8,128)(2,1)S(1)} fusion(pred[12,6,256]{1,0,2:T(8,128)(4,1)S(1)} %and.62, s32[12,6]{1,0:T(8,128)S(1)} %eq.76, s32[256]{0:T(256)S(1)} %add.146), kind=kLoop, calls=%fused_computation.29 | loop fusion | flops 70656 | bytes 25888 | tf_op jit(solution)/shard_map/reduce_max | solution.py:175
  39.0 0.5 convolution_convert_fusion.1
  39.5 1.5 %reshape.309 = bf16[128,2,2048]{2,1,0:T(2,128)(2,1)} reshape(bf16[256,2048]{1,0:T(8,128)(2,1)S(1)} %convolution_convert_fusion.1) | data formatting | bytes 2097152 | tf_op jit(solution)/shard_map/reshape | solution.py:182
  41.0 30.1 %all_to_all.10 = bf16[128,2,2048]{2,1,0:T(2,128)(2,1)S(1)} all-to-all(bf16[128,2,2048]{2,1,0:T(2,128)(2,1)} %reshape.309), channel_id=1, replica_groups=mesh['ep'=128] {'ep'}, dimensions={0} | all-to-all | bytes 2097152 | tf_op jit(solution)/shard_map/all_to_all | solution.py:181
  71.1 2.7 %collective-permute-done = bf16[128,2,2048]{2,1,0:T(2,128)(2,1)S(1)} collective-permute-done((bf16[128,2,2048]{2,1,0:T(2,128)(2,1)S(1)}, bf16[128,2,2048]{2,1,0:T(2,128)(2,1)S(1)}, u32[]{:S(2)}, u32[]{:S(2)}) %collective-permute-start) | collective-permute-done | bytes 1048608 | tf_op jit(solution)/shard_map/ppermute | solution.py:24
  73.8 3.2 %pad_maximum_fusion = bf16[128,4,2048]{2,1,0:T(4,128)(2,1)} fusion(bf16[128,2,2048]{2,1,0:T(2,128)(2,1)S(1)} %collective-permute-done, bf16[128,2,2048]{2,1,0:T(2,128)(2,1)S(1)} %all_to_all.10), kind=kLoop, calls=%fused_computation.27 | loop fusion | flops 4194304 | bytes 4194304 | tf_op jit(solution)/shard_map/concatenate | solution.py:189
  77.0 4.0 %reshape.310 = bf16[512,2048]{1,0:T(8,128)(2,1)} reshape(bf16[128,4,2048]{2,1,0:T(4,128)(2,1)} %pad_maximum_fusion) | data formatting | bytes 4194304 | tf_op jit(solution)/shard_map/reshape | solution.py:190
  81.0 3.1 %fusion.31 = f32[512,256]{1,0:T(8,128)} fusion(bf16[512,2048]{1,0:T(8,128)(2,1)} %reshape.310, bf16[1,2048,256]{2,1,0:T(8,128)(2,1)S(1)} %copy-done.15), kind=kOutput, calls=%fused_computation.41 | convolution fusion | flops 536870912 | bytes 3670016 | tf_op jit(solution)/shard_map/dot_general | solution.py:193
  84.1 5.9 %convolution_convert_fusion = bf16[512,2048]{1,0:T(8,128)(2,1)} fusion(bf16[1,256,2048]{2,1,0:T(8,128)(2,1)} %param.41, f32[512,256]{1,0:T(8,128)} %fusion.31, bf16[512,2048]{1,0:T(8,128)(2,1)} %reshape.310, bf16[1,2048,256]{2,1,0:T(8,128)(2,1)} %param.39), kind=kOutput, calls=%fused_computation.21 | convolution fusion | flops 1075576832 | bytes 6815744 | tf_op jit(solution)/shard_map/dot_general | solution.py:196
  90.0 4.1 %reshape.311 = bf16[128,4,2048]{2,1,0:T(4,128)(2,1)} reshape(bf16[512,2048]{1,0:T(8,128)(2,1)} %convolution_convert_fusion) | data formatting | bytes 4194304 | tf_op jit(solution)/shard_map/reshape | solution.py:198
  94.2 2.9 %slice.38 = bf16[128,2,2048]{2,1,0:T(2,128)(2,1)S(1)} slice(bf16[128,4,2048]{2,1,0:T(4,128)(2,1)} %reshape.311), slice={[0:128], [2:4], [0:2048]} | slice | bytes 2097152 | tf_op jit(solution)/shard_map/slice | solution.py:200
  97.1 0.2 collective-permute-start.1
  97.3 2.5 %collective-permute-done.1 = bf16[128,2,2048]{2,1,0:T(2,128)(2,1)S(1)} collective-permute-done((bf16[128,2,2048]{2,1,0:T(2,128)(2,1)S(1)}, bf16[128,2,2048]{2,1,0:T(2,128)(2,1)S(1)}, u32[]{:S(2)}, u32[]{:S(2)}) %collective-permute-start.1) | collective-permute-done | bytes 1048608 | tf_op jit(solution)/shard_map/ppermute | solution.py:24
  99.8 2.1 %convert_add_fusion = bf16[128,2,2048]{2,1,0:T(2,128)(2,1)} fusion(bf16[128,2,2048]{2,1,0:T(2,128)(2,1)S(1)} %collective-permute-done.1, bf16[128,4,2048]{2,1,0:T(4,128)(2,1)S(1)} %copy-done.2), kind=kLoop, calls=%fused_computation.28 | loop fusion | flops 2097152 | bytes 3145728 | tf_op jit(solution)/shard_map/add | solution.py:201
  101.9 4.8 %all-to-all-start.1 = ((bf16[128,2,2048]{2,1,0:T(2,128)(2,1)}), bf16[128,2,2048]{2,1,0:T(2,128)(2,1)S(1)}, u32[]{:S(2)}, u32[]{:S(2)}) async-start(bf16[128,2,2048]{2,1,0:T(2,128)(2,1)} %convert_add_fusion), calls=%async_computation.1 | async-start | bytes 2097152 | tf_op jit(solution)/shard_map/all_to_all | solution.py:202
  106.7 0.1 broadcast_add_fusion
  106.8 0.2 compare_and_fusion
  107.0 1.8 %and.61 = pred[12,6,256]{1,0,2:T(8,128)(4,1)} reshape(pred[72,128,2]{0,2,1:T(4,128)(4,1)S(1)} %compare_and_fusion) | data formatting | bytes 36864 | tf_op jit(solution)/shard_map/and | solution.py:171
  108.8 0.1 copy.54
  108.9 0.7 pad_maximum_fusion.2
  109.6 16.3 %all-to-all-done.1 = bf16[128,2,2048]{2,1,0:T(2,128)(2,1)S(1)} async-done(((bf16[128,2,2048]{2,1,0:T(2,128)(2,1)}), bf16[128,2,2048]{2,1,0:T(2,128)(2,1)S(1)}, u32[]{:S(2)}, u32[]{:S(2)}) %all-to-all-start.1) | async-done | bytes 1048608 | tf_op jit(solution)/shard_map/all_to_all | solution.py:202
  125.8 1.2 reshape.317
  127.0 2.2 %fusion.21 = f32[12,2048]{1,0:T(8,128)S(1)} fusion(bf16[256,2048,1]{1,0,2:T(8,128)(2,1)} %reshape.317, pred[12,6,256]{1,0,2:T(8,128)(4,1)} %and.61, f32[12,6]{1,0:T(8,128)S(1)} %copy.54), kind=kOutput, calls=%fused_computation.31 | convolution fusion | flops 75767808 | bytes 1165600 | tf_op jit(solution)/shard_map/dot_general | solution.py:203
  129.2 0.7 add.150
  (63 shorter events, 0.7 us)
Async XLA Ops:
  0.6 3.7 %copy-start = (bf16[2048,512]{1,0:T(8,128)(2,1)S(1)}, bf16[2048,512]{1,0:T(8,128)(2,1)}, u32[]{:S(2)}) copy-start(bf16[2048,512]{1,0:T(8,128)(2,1)} %param.33) | copy-start | bytes 6291460
  0.6 5.8 %copy-start.4 = (bf16[12,2048]{1,0:T(8,128)(2,1)S(1)}, bf16[12,2048]{1,0:T(8,128)(2,1)}, u32[]{:S(2)}) copy-start(bf16[12,2048]{1,0:T(8,128)(2,1)} %param.22) | copy-start | bytes 147460
  0.7 5.8 %copy-start.7 = (f32[2048]{0:T(1024)S(1)}, f32[2048]{0:T(1024)}, u32[]{:S(2)}) copy-start(f32[2048]{0:T(1024)} %param.28) | copy-start | bytes 24580
  0.7 5.0 %copy-start.10 = (f32[512]{0:T(512)S(1)}, f32[512]{0:T(512)}, u32[]{:S(2)}) copy-start(f32[512]{0:T(512)} %param.30) | copy-start | bytes 6148
  4.3 4.5 %copy-start.13 = (f32[512]{0:T(512)S(1)}, f32[512]{0:T(512)}, u32[]{:S(2)}) copy-start(f32[512]{0:T(512)} %param.29) | copy-start | bytes 6148
  5.9 6.4 %copy-start.6 = (bf16[12,512]{1,0:T(8,128)(2,1)}, bf16[12,512]{1,0:T(8,128)(2,1)S(1)}, u32[]{:S(2)}) copy-start(bf16[12,512]{1,0:T(8,128)(2,1)S(1)} %multiply_convert_fusion.4) | copy-start | bytes 36868
  6.5 2.3 %copy-start.3 = (bf16[512,1536]{1,0:T(8,128)(2,1)S(1)}, bf16[512,1536]{1,0:T(8,128)(2,1)}, u32[]{:S(2)}) copy-start(bf16[512,1536]{1,0:T(8,128)(2,1)} %param.35) | copy-start | bytes 4718596
  6.5 4.0 %copy-start.5 = (bf16[512,1024]{1,0:T(8,128)(2,1)S(1)}, bf16[512,1024]{1,0:T(8,128)(2,1)}, u32[]{:S(2)}) copy-start(bf16[512,1024]{1,0:T(8,128)(2,1)} %param.36) | copy-start | bytes 3145732
  8.8 3.5 %copy-start.8 = (s32[12]{0:T(128)S(1)}, s32[12]{0:T(128)}, u32[]{:S(2)}) copy-start(s32[12]{0:T(128)} %param.25) | copy-start | bytes 148
  12.4 4.7 %copy-start.1 = (bf16[12,1024,64]{1,2,0:T(8,128)(2,1)S(1)}, bf16[12,1024,64]{1,2,0:T(8,128)(2,1)}, u32[]{:S(2)}) copy-start(bf16[12,1024,64]{1,2,0:T(8,128)(2,1)} %get-tuple-element.243) | copy-start | bytes 4718596 | tf_op jit(solution)/shard_map/while
  21.4 4.7 %copy-start.1 = (bf16[12,1024,64]{1,2,0:T(8,128)(2,1)S(1)}, bf16[12,1024,64]{1,2,0:T(8,128)(2,1)}, u32[]{:S(2)}) copy-start(bf16[12,1024,64]{1,2,0:T(8,128)(2,1)} %get-tuple-element.243) | copy-start | bytes 4718596 | tf_op jit(solution)/shard_map/while
  32.1 3.0 %copy-start.11 = (s32[12,6]{0,1:T(8,128)S(1)}, s32[12,6]{0,1:T(8,128)}, u32[]{:S(2)}) copy-start(s32[12,6]{0,1:T(8,128)} %param.26) | copy-start | bytes 868
  32.1 3.6 %copy-start.14 = (s32[128]{0:T(128)S(1)}, s32[128]{0:T(128)}, u32[]{:S(2)}) copy-start(s32[128]{0:T(128)} %and_select_fusion.1) | copy-start | bytes 1540
  32.1 6.9 %copy-start.9 = (f32[2048]{0:T(1024)S(1)}, f32[2048]{0:T(1024)}, u32[]{:S(2)}) copy-start(f32[2048]{0:T(1024)} %param.31) | copy-start | bytes 24580
  71.1 2.7 %collective-permute-start = (bf16[128,2,2048]{2,1,0:T(2,128)(2,1)S(1)}, bf16[128,2,2048]{2,1,0:T(2,128)(2,1)S(1)}, u32[]{:S(2)}, u32[]{:S(2)}) collective-permute-start(bf16[128,2,2048]{2,1,0:T(2,128)(2,1)S(1)} %all_to_all.10), channel_id=1, source_target_pairs={{0,1},{1,0},{2,3},{3,2},{4,5},{5,4},{6,7},{7,6},{8,9},{9,8},{10,11... | collective-permute-start | bytes 3145736 | tf_op jit(solution)/shard_map/ppermute | solution.py:24
  76.9 4.0 %copy-start.15 = (bf16[1,2048,256]{2,1,0:T(8,128)(2,1)S(1)}, bf16[1,2048,256]{2,1,0:T(8,128)(2,1)}, u32[]{:S(2)}) copy-start(bf16[1,2048,256]{2,1,0:T(8,128)(2,1)} %param.40) | copy-start | bytes 3145732
  94.2 5.7 %copy-start.2 = (bf16[128,4,2048]{2,1,0:T(4,128)(2,1)S(1)}, bf16[128,4,2048]{2,1,0:T(4,128)(2,1)}, u32[]{:S(2)}) copy-start(bf16[128,4,2048]{2,1,0:T(4,128)(2,1)} %reshape.311) | copy-start | bytes 6291460
  97.1 2.7 %collective-permute-start.1 = (bf16[128,2,2048]{2,1,0:T(2,128)(2,1)S(1)}, bf16[128,2,2048]{2,1,0:T(2,128)(2,1)S(1)}, u32[]{:S(2)}, u32[]{:S(2)}) collective-permute-start(bf16[128,2,2048]{2,1,0:T(2,128)(2,1)S(1)} %slice.38), channel_id=1, source_target_pairs={{0,1},{1,0},{2,3},{3,2},{4,5},{5,4},{6,7},{7,6},{8,9},{9,8},{10,11... | collective-permute-start | bytes 3145736 | tf_op jit(solution)/shard_map/ppermute | solution.py:24
  101.9 6.9 %copy-start.12 = (f32[12,6]{0,1:T(8,128)S(1)}, f32[12,6]{0,1:T(8,128)}, u32[]{:S(2)}) copy-start(f32[12,6]{0,1:T(8,128)} %param.27) | copy-start | bytes 868
  101.9 23.9 %all-to-all-start.1 = ((bf16[128,2,2048]{2,1,0:T(2,128)(2,1)}), bf16[128,2,2048]{2,1,0:T(2,128)(2,1)S(1)}, u32[]{:S(2)}, u32[]{:S(2)}) async-start(bf16[128,2,2048]{2,1,0:T(2,128)(2,1)} %convert_add_fusion), calls=%async_computation.1 | async-start | bytes 2097152 | tf_op jit(solution)/shard_map/all_to_all | solution.py:202
where the time goes:
time: 131 us; the launch traced here: 130 us
  matrix products  39.4 us (30%)
  blocking collectives  30.1 us (23%)
  waiting for transfers between devices  21.4 us (16%)
  local copies, waits for them, and re-layouts  17.7 us (14%)
  other arithmetic  14.5 us (11%)
  starting transfers between devices  4.98 us (4%)
  between operations  1.69 us (1%)
    all_to_all x1, blocking collectives, mix_experts(): lax.all_to_all(outgoing.reshape(half_count, per_core, model_width), 'ep',...  30.1 us
    all_to_all x1, waiting for transfers between devices, mix_experts(): lax.all_to_all(pair_sum, 'ep', split_axis=0, concat_axis=0, tiled=True)  16.3 us
    dot_general x2, matrix products, block_step(): jnp.einsum('thc,tpc->thp', q_latent, latent_block, preferred_element_type...  9.26 us
    dot_general x2, matrix products, block_step(): jnp.einsum('thp,tpc->thc', block_probs.astype(jnp.bfloat16), latent_block...  7.5 us
    dot_general x1, matrix products, mix_experts(): jnp.dot(hidden, down_half, preferred_element_type=jnp.float32)  5.94 us
    ppermute x2, waiting for transfers between devices, partner(): return lax.ppermute(value, axis, pairs)  5.18 us
    all_to_all x1, starting transfers between devices, mix_experts(): lax.all_to_all(pair_sum, 'ep', split_axis=0, concat_axis=0, tiled=True)  4.76 us
    reshape x1, local copies, waits for them, and re-layouts, mix_experts(): outputs = jnp.dot(hidden, down_half, preferred_element_type=jnp.float32)....  4.11 us
  transfers between devices with their start and end apart: 3, of which 3 were waited for; matrix products, arithmetic and copies ran while one was open for 2% of the time, Pallas kernels for 0%

commit v1 on v0

v1 whole, which is shorter than its diff:
```python
import jax
import jax.numpy as jnp
import numpy as np
from jax import lax
from jax.experimental import pallas as pl
from jax.experimental.pallas import tpu as pltpu
from jax.sharding import PartitionSpec as P

HEADS = 8
KV_RANK = 512
NOPE_DIM = 128
ROPE_DIM = 64
TOP_K = 6
SEQ_DEV = 12
CACHE = 1024
D = 2048
CAPACITY = 3
SIDE = 4
CHIPS = 64
CHUNKS = 4
PER_CHUNK = CHIPS // CHUNKS
ROWS = PER_CHUNK * CAPACITY
SLOTS = CHIPS * CAPACITY
LANES = 128
TILES = D // LANES
PARTS = KV_RANK // LANES
EPS = 1e-06
THETA = 10000.0
F32 = jnp.float32
BF16 = jnp.bfloat16


def norm_gain(values, gain):
    return values * lax.rsqrt(jnp.mean(values * values, axis=-1, keepdims=True) + EPS) * gain


def dot(a, b):
    return jnp.dot(a, b, preferred_element_type=F32)


def dot_t(a, b):
    return lax.dot_general(a, b, (((1,), (1,)), ((), ())), preferred_element_type=F32)


def swap_halves(v):
    half = ROPE_DIM // 2
    return jnp.concatenate([v[:, half:], v[:, :half]], axis=1)


def chip_at(x, y, z):
    return z * (SIDE * SIDE) + y * SIDE + x


def wrap(v):
    return lax.rem(v + 2 * SIDE, SIDE)


def offset_of(p):
    chunk = p // PER_CHUNK
    dx = lax.rem(p, SIDE)
    dy = lax.rem(p // SIDE, SIDE)
    return dx, dy, wrap(chunk - dx - dy)


def kernel(
    len_s, weight_s, tok, ag, qg, kg, mg, ids, inv,
    cache, rope_t, qdown, kvdown, krope_t, qup, kup, vup, wout, gate, up, down,
    mixed_o, latent_o, key_o,
    cache_v, rope_v, qdown_v, kvdown_v, krope_v, qup_v, kup_v, vup_v, wout_v,
    gate_v, up_v, down_v,
    qlat, qrope, scores, olat, own_v, table_v, slot_v, table_s, slot_s,
    tile_f, attn_f, rows_b, send_b, recv_b, out_b, back_b, x_b,
    w_sem, cache_sem, rope_sem, e_sem, s_sem, x_send, x_recv,
    d_send, d_recv, r_send, r_recv,
):
    me = lax.axis_index("ep")
    core = lax.rem(me, 2)
    chip = me // 2
    mx = lax.rem(chip, SIDE)
    my = lax.rem(chip // SIDE, SIDE)
    mz = chip // (SIDE * SIDE)
    sibling = me + 1 - 2 * core

    def target(p, sign):
        dx, dy, dz = offset_of(p)
        there = chip_at(wrap(mx + sign * dx), wrap(my + sign * dy), wrap(mz + sign * dz))
        return there

    barrier = pltpu.get_barrier_semaphore()

    weights = [
        (qdown, qdown_v), (qup, qup_v), (kup, kup_v), (kvdown, kvdown_v), (krope_t, krope_v),
        (vup, vup_v), (wout, wout_v),
    ]
    w_copy = [
        pltpu.make_async_copy(src, dst, w_sem.at[i]) for i, (src, dst) in enumerate(weights)
    ]
    experts = [(gate, gate_v), (up, up_v), (down, down_v)]
    e_copy = [
        pltpu.make_async_copy(src.at[0], dst.at[0], e_sem.at[i])
        for i, (src, dst) in enumerate(experts)
    ]

    def cache_copies(t):
        return (
            pltpu.make_async_copy(cache.at[t], cache_v.at[t], cache_sem.at[t]),
            pltpu.make_async_copy(rope_t.at[t], rope_v.at[t], rope_sem.at[t]),
        )

    def start_cache(t):
        for c in cache_copies(t):
            c.start()

    for i in range(5):
        w_copy[i].start()
    for t in range(6):
        start_cache(t)

    def greet(p, carry):
        pl.semaphore_signal(
            barrier, inc=1, device_id=(target(p, 1) * 2 + core,),
            device_id_type=pl.DeviceIdType.MESH,
        )
        return carry

    lax.fori_loop(1, CHIPS, greet, 0)
    pl.semaphore_signal(
        barrier, inc=1, device_id=(sibling,), device_id_type=pl.DeviceIdType.MESH
    )

    ids_v = ids[...]
    table_v[...] = jnp.zeros((8, LANES), jnp.int32)
    slot_v[...] = jnp.zeros((8, LANES), jnp.int32)
    expert_iota = lax.broadcasted_iota(jnp.int32, (LANES, SEQ_DEV), 0)
    hits = jnp.zeros((LANES, SEQ_DEV), F32)
    for k in range(TOP_K):
        hits = jnp.where(expert_iota == ids_v[k : k + 1, :], 1.0, hits)
    before = jnp.where(
        lax.broadcasted_iota(jnp.int32, (SEQ_DEV, SEQ_DEV), 0)
        < lax.broadcasted_iota(jnp.int32, (SEQ_DEV, SEQ_DEV), 1),
        1.0,
        0.0,
    )
    rank = dot(hits.astype(BF16), before.astype(BF16))
    token_less = (
        lax.broadcasted_iota(jnp.int32, (8, SEQ_DEV), 1).astype(F32) - SEQ_DEV
    ).astype(BF16)
    row_iota = lax.broadcasted_iota(jnp.int32, (8, LANES), 0)
    table = jnp.zeros((8, LANES), F32)
    for s in range(CAPACITY):
        chosen = jnp.where(rank == float(s), hits, 0.0).astype(BF16)
        table = jnp.where(row_iota == s, dot_t(token_less, chosen) + SEQ_DEV, table)
    table_v[...] = jnp.clip(table.astype(jnp.int32), 0, SEQ_DEV)
    for k in range(TOP_K):
        e = ids_v[k : k + 1, :]
        own_rank = jnp.sum(jnp.where(expert_iota == e, rank, 0.0), axis=0, keepdims=True)
        dx = ((e & 3) - mx) & 3
        dy = (((e >> 2) & 3) - my) & 3
        dz = ((e >> 4) - mz) & 3
        place = ((dx + dy + dz) & 3) * PER_CHUNK + dx + SIDE * dy
        slot_v[k : k + 1, 0:SEQ_DEV] = place * CAPACITY + jnp.clip(
            own_rank.astype(jnp.int32), 0, CAPACITY - 1
        )
    table_copy = pltpu.make_async_copy(table_v, table_s, s_sem.at[0])
    slot_copy = pltpu.make_async_copy(slot_v, slot_s, s_sem.at[1])
    table_copy.start()
    slot_copy.start()

    row16 = lax.broadcasted_iota(jnp.int32, (16, ROPE_DIM), 0)
    length_col = jnp.zeros((16, ROPE_DIM), F32)
    for t in range(SEQ_DEV):
        length_col = jnp.where(row16 == t, len_s[t].astype(F32), length_col)
    angles = length_col * inv[0:1, 0:ROPE_DIM]
    cosine = jnp.cos(angles)[0:SEQ_DEV]
    first_half = lax.broadcasted_iota(jnp.int32, (16, ROPE_DIM), 1) < ROPE_DIM // 2
    sine = jnp.sin(angles)
    sine = jnp.where(first_half, -sine, sine)[0:SEQ_DEV]

    normed = norm_gain(tok[...].astype(F32), ag[...]).astype(BF16)
    w_copy[0].wait()
    q_low = norm_gain(dot(normed, qdown_v[...]), qg[...]).astype(BF16)
    w_copy[1].wait()
    query = dot(q_low, qup_v[...])
    w_copy[2].wait()
    head_width = NOPE_DIM + ROPE_DIM
    zeros64 = jnp.zeros((SEQ_DEV, LANES - ROPE_DIM), F32)
    for h in range(HEADS):
        nope = query[:, h * head_width : h * head_width + NOPE_DIM].astype(BF16)
        lat = dot_t(nope, kup_v[:, h * NOPE_DIM : (h + 1) * NOPE_DIM])
        for j in range(PARTS):
            qlat[j, pl.ds(h, SEQ_DEV, stride=HEADS), :] = lat[:, j * LANES : (j + 1) * LANES]
        rot = query[:, h * head_width + NOPE_DIM : (h + 1) * head_width]
        rot = rot * cosine + swap_halves(rot) * sine
        qrope[pl.ds(h, SEQ_DEV, stride=HEADS), :] = jnp.concatenate([rot, zeros64], axis=1)
    w_copy[3].wait()
    new_latent = norm_gain(dot(normed, kvdown_v[...]), kg[...]).astype(BF16)
    latent_o[...] = new_latent
    w_copy[4].wait()
    new_key = dot_t(normed, krope_v[...])
    new_key = (new_key * cosine + swap_halves(new_key) * sine).astype(BF16)
    key_o[...] = new_key
    own_all = jnp.concatenate([new_latent.astype(F32), new_key.astype(F32), zeros64], axis=1)
    for t in range(SEQ_DEV):
        own_v[t] = own_all[t : t + 1, :]

    scale = (NOPE_DIM + ROPE_DIM) ** (-0.5)
    position = lax.broadcasted_iota(jnp.int32, (HEADS, CACHE), 1)

    def rows_of(t):
        return pl.ds(pl.multiple_of(t * HEADS, HEADS), HEADS)

    def query_of(t):
        parts = [qlat[j, rows_of(t), :] for j in range(PARTS)]
        return jnp.concatenate(parts, axis=1).astype(BF16)

    def score_step(t):
        for c in cache_copies(t):
            c.wait()
        q = query_of(t)
        r = qrope[rows_of(t), :].astype(BF16)[:, :ROPE_DIM]
        s = (dot_t(q, cache_v[t]) + dot(r, rope_v[t])) * scale
        scores[rows_of(t), :] = jnp.where(position < len_s[t], s, -jnp.inf)

    def value_step(t):
        q = query_of(t).astype(F32)
        r = qrope[rows_of(t), :].astype(BF16).astype(F32)
        own_row = own_v[t]
        own_latent = own_row[:, 0:KV_RANK]
        own_key = own_row[:, KV_RANK : KV_RANK + LANES]
        own = (
            jnp.sum(q * own_latent, axis=1, keepdims=True)
            + jnp.sum(r * own_key, axis=1, keepdims=True)
        ) * scale
        s = scores[rows_of(t), :]
        peak = jnp.maximum(jnp.max(s, axis=1, keepdims=True), own)
        probs = jnp.exp(s - peak)
        own_prob = jnp.exp(own - peak)
        denom = jnp.sum(probs, axis=1, keepdims=True) + own_prob
        total = dot(probs.astype(BF16), cache_v[t])
        total = total + own_prob.astype(BF16).astype(F32) * own_latent
        total = total / denom
        for j in range(PARTS):
            olat[j, rows_of(t), :] = total[:, j * LANES : (j + 1) * LANES]

    score_step(0)
    score_step(1)

    def body(i, carry):
        start_cache(2 * i + 4)
        start_cache(2 * i + 5)
        score_step(2 * i)
        score_step(2 * i + 1)
        value_step(2 * i - 2)
        value_step(2 * i - 1)
        return carry

    lax.fori_loop(1, 3, body, 0)
    for c in e_copy:
        c.start()
    lax.fori_loop(3, 4, body, 0)
    w_copy[5].start()
    w_copy[6].start()

    def tail(i, carry):
        score_step(2 * i)
        score_step(2 * i + 1)
        value_step(2 * i - 2)
        value_step(2 * i - 1)
        return carry

    lax.fori_loop(4, 5, tail, 0)
    pl.semaphore_wait(barrier, CHIPS)
    swap = []
    for i, (_, dst) in enumerate(experts):
        e_copy[i].wait()
        swap.append(
            pltpu.make_async_remote_copy(
                src_ref=dst.at[0],
                dst_ref=dst.at[1],
                send_sem=x_send.at[i],
                recv_sem=x_recv.at[i],
                device_id=(sibling,),
                device_id_type=pl.DeviceIdType.MESH,
            )
        )
        swap[-1].start()
    lax.fori_loop(5, 6, tail, 0)
    value_step(10)
    value_step(11)

    w_copy[5].wait()
    heads = []
    for h in range(HEADS):
        parts = [olat[j, pl.ds(h, SEQ_DEV, stride=HEADS), :] for j in range(PARTS)]
        o = jnp.concatenate(parts, axis=1).astype(BF16)
        heads.append(dot(o, vup_v[:, h * LANES : (h + 1) * LANES]).astype(BF16))
    heads_out = jnp.concatenate(heads, axis=1)
    w_copy[6].wait()
    mixed_attn = (tok[...].astype(F32) + dot(heads_out, wout_v[...])).astype(BF16).astype(F32)
    moe_in = norm_gain(mixed_attn, mg[...])
    for j in range(TILES):
        cols = slice(j * LANES, (j + 1) * LANES)
        tile_f[pl.ds(j, SEQ_DEV, stride=TILES), :] = moe_in[:, cols]
        attn_f[pl.ds(j, SEQ_DEV, stride=TILES), :] = mixed_attn[:, cols]
    rows_b[0:SEQ_DEV] = (
        tile_f[0 : SEQ_DEV * TILES, :].reshape(SEQ_DEV, TILES, LANES).astype(BF16)
    )
    rows_b[SEQ_DEV] = jnp.zeros((TILES, LANES), BF16)

    table_copy.wait()
    slot_copy.wait()

    for s in range(CAPACITY):
        recv_b[s] = rows_b[table_s[s, chip]]

    def fill(p, carry):
        there = target(p, 1)
        for s in range(CAPACITY):
            send_b[p * CAPACITY + s] = rows_b[table_s[s, there]]
        return carry

    lax.fori_loop(1, CHIPS, fill, 0)

    def block(ref, p, count=1):
        return ref.at[pl.ds(p * CAPACITY, count * CAPACITY)]

    def dispatch(p):
        return pltpu.make_async_remote_copy(
            src_ref=block(send_b, p),
            dst_ref=block(recv_b, p),
            send_sem=d_send,
            recv_sem=d_recv.at[p // PER_CHUNK],
            device_id=(target(p, 1) * 2 + core,),
            device_id_type=pl.DeviceIdType.MESH,
        )

    def go_back(p):
        return pltpu.make_async_remote_copy(
            src_ref=block(out_b, p),
            dst_ref=block(back_b, p),
            send_sem=r_send,
            recv_sem=r_recv,
            device_id=(target(p, -1) * 2 + core,),
            device_id_type=pl.DeviceIdType.MESH,
        )

    def start_dispatch(p, carry):
        dispatch(p).start()
        return carry

    lax.fori_loop(1, CHIPS, start_dispatch, 0)
    for c in swap:
        c.wait()

    def expert_chunk(c):
        first = 1 if c == 0 else 0
        count = PER_CHUNK - first
        landed = block(recv_b, c * PER_CHUNK + first, count)
        pltpu.make_async_copy(landed, landed, d_recv.at[c]).wait()
        x = recv_b[c * ROWS : (c + 1) * ROWS].astype(F32)
        tile_f[...] = x.reshape(ROWS * TILES, LANES)
        for j in range(TILES):
            x_b[:, j * LANES : (j + 1) * LANES] = tile_f[
                pl.ds(j, ROWS, stride=TILES), :
            ].astype(BF16)
        xv = x_b[...]
        total = None
        for half in range(2):
            g = dot(xv, gate_v[half])
            u = dot(xv, up_v[half])
            hidden = (g / (1.0 + jnp.exp(-g)) * u).astype(BF16)
            part = dot(hidden, down_v[half])
            total = part if total is None else total + part
        for j in range(TILES):
            tile_f[pl.ds(j, ROWS, stride=TILES), :] = total[:, j * LANES : (j + 1) * LANES]
        out = tile_f[...].reshape(ROWS, TILES, LANES).astype(BF16)
        if c == 0:
            back_b[0:CAPACITY] = out[0:CAPACITY]
        out_b[c * ROWS : (c + 1) * ROWS] = out

        def start_back(p, carry):
            go_back(p).start()
            return carry

        lax.fori_loop(c * PER_CHUNK + first, (c + 1) * PER_CHUNK, start_back, 0)

    for c in range(CHUNKS):
        expert_chunk(c)

    others = block(back_b, 1, CHIPS - 1)
    pltpu.make_async_copy(others, others, r_recv).wait()
    for t in range(SEQ_DEV):
        acc = attn_f[t * TILES : (t + 1) * TILES, :]
        for k in range(TOP_K):
            acc = acc + weight_s[k, t] * back_b[slot_s[k, t]].astype(F32)
        mixed_o[t] = acc
    sent = block(send_b, 1, CHIPS - 1)
    pltpu.make_async_copy(sent, sent, d_send).wait()
    pltpu.make_async_copy(sent, sent, r_send).wait()


def shards(
    tokens, cache_latent, cache_rope, cache_lengths, expert_ids, route_weight,
    attn_gain, q_gain, kv_gain, moe_gain,
    w_qdown, w_kvdown, w_krope, w_qup, w_kup, w_vup, w_out,
    expert_gate, expert_up, expert_down,
):
    half = ROPE_DIM // 2
    inverse = np.float32(THETA) ** (-np.arange(half, dtype=np.float32) / np.float32(half))
    inverse = jnp.asarray(np.tile(inverse, LANES // half)[None, :].astype(np.float32))
    smem = pl.BlockSpec(memory_space=pltpu.SMEM)
    vmem = pl.BlockSpec(memory_space=pltpu.VMEM)
    anywhere = pl.BlockSpec(memory_space=pl.ANY)
    dma = pltpu.SemaphoreType.DMA
    scratch = [
        pltpu.VMEM((SEQ_DEV, CACHE, KV_RANK), BF16),
        pltpu.VMEM((SEQ_DEV, ROPE_DIM, CACHE), BF16),
        pltpu.VMEM((D, 512), BF16),
        pltpu.VMEM((D, KV_RANK), BF16),
        pltpu.VMEM((ROPE_DIM, D), BF16),
        pltpu.VMEM((512, 1536), BF16),
        pltpu.VMEM((KV_RANK, 1024), BF16),
        pltpu.VMEM((KV_RANK, 1024), BF16),
        pltpu.VMEM((1024, D), BF16),
        pltpu.VMEM((2, D, 256), BF16),
        pltpu.VMEM((2, D, 256), BF16),
        pltpu.VMEM((2, 256, D), BF16),
        pltpu.VMEM((PARTS, SEQ_DEV * HEADS, LANES), F32),
        pltpu.VMEM((SEQ_DEV * HEADS, LANES), F32),
        pltpu.VMEM((SEQ_DEV * HEADS, CACHE), F32),
        pltpu.VMEM((PARTS, SEQ_DEV * HEADS, LANES), F32),
        pltpu.VMEM((SEQ_DEV, 1, KV_RANK + LANES), F32),
        pltpu.VMEM((8, LANES), jnp.int32),
        pltpu.VMEM((8, LANES), jnp.int32),
        pltpu.SMEM((8, LANES), jnp.int32),
        pltpu.SMEM((8, LANES), jnp.int32),
        pltpu.VMEM((ROWS * TILES, LANES), F32),
        pltpu.VMEM((SEQ_DEV * TILES, LANES), F32),
        pltpu.VMEM((SEQ_DEV + 1, TILES, LANES), BF16),
        pltpu.VMEM((SLOTS, TILES, LANES), BF16),
        pltpu.VMEM((SLOTS, TILES, LANES), BF16),
        pltpu.VMEM((SLOTS, TILES, LANES), BF16),
        pltpu.VMEM((SLOTS, TILES, LANES), BF16),
        pltpu.VMEM((ROWS, D), BF16),
        dma((7,)), dma((SEQ_DEV,)), dma((SEQ_DEV,)), dma((3,)), dma((2,)),
        dma((3,)), dma((3,)),
        dma, dma((CHUNKS,)), dma, dma,
    ]
    mixed, latent, key = pl.pallas_call(
        kernel,
        out_shape=(
            jax.ShapeDtypeStruct((SEQ_DEV, TILES, LANES), F32),
            jax.ShapeDtypeStruct((SEQ_DEV, KV_RANK), BF16),
            jax.ShapeDtypeStruct((SEQ_DEV, ROPE_DIM), BF16),
        ),
        in_specs=[smem, smem] + [vmem] * 7 + [anywhere] * 12,
        out_specs=(vmem, vmem, vmem),
        scratch_shapes=scratch,
        compiler_params=pltpu.CompilerParams(
            collective_id=0, has_side_effects=True, vmem_limit_bytes=60 * 1024 * 1024
        ),
        name="layer",
    )(
        cache_lengths, route_weight.T, tokens,
        attn_gain[None, :], q_gain[None, :], kv_gain[None, :], moe_gain[None, :],
        expert_ids.T, inverse,
        cache_latent, jnp.swapaxes(cache_rope, 1, 2),
        w_qdown, w_kvdown, w_krope.T, w_qup, w_kup, w_vup, w_out,
        expert_gate, expert_up, expert_down,
    )
    return (mixed.reshape(SEQ_DEV, D), latent, key)


def solution(mesh):
    rows = P("ep", None)
    cube = P("ep", None, None)
    placed = (rows, cube, cube, P("ep"), rows, rows) + (P(),) * 11 + (cube, cube, cube)
    return jax.shard_map(
        shards,
        mesh=mesh,
        in_specs=placed,
        out_specs=(rows, rows, rows),
        check_vma=False,
    )
```

time: 131 us -> 49.2 us (0.38)
  Pallas kernels: 0 us -> 44.1 us
  matrix products: 39.4 us -> 0 us
  blocking collectives: 30.1 us -> 0 us
  waiting for transfers between devices: 21.4 us -> 0 us
  other arithmetic: 14.5 us -> 0 us
  local copies, waits for them, and re-layouts: 17.7 us -> 4.19 us
  starting transfers between devices: 4.98 us -> 0 us
    pallas_call x0 -> x1, Pallas kernels: none -> 44.1 us  [shards(): pl.pallas_call(kernel, out_shape=(jax.ShapeDtypeStruct((SEQ_DEV, TILES, L...]
    dot_general x19 -> x0, matrix products: 39.4 us -> none  [the longest x2 9.26 us: block_step(): jnp.einsum('thc,tpc->thp', q_latent, latent_block, preferred_element_type...]
    all_to_all x1 -> x0, blocking collectives: 30.1 us -> none  [mix_experts(): lax.all_to_all(outgoing.reshape(half_count, per_core, model_width), 'ep',...]
    all_to_all x1 -> x0, waiting for transfers between devices: 16.3 us -> none  [mix_experts(): lax.all_to_all(pair_sum, 'ep', split_axis=0, concat_axis=0, tiled=True)]
    reshape x5 -> x0, local copies, waits for them, and re-layouts: 11 us -> none  [the longest x1 4.11 us: mix_experts(): outputs = jnp.dot(hidden, down_half, preferred_element_type=jnp.float32)....]
    ppermute x2 -> x0, waiting for transfers between devices: 5.18 us -> none  [partner(): return lax.ppermute(value, axis, pairs)]
    all_to_all x1 -> x0, starting transfers between devices: 4.76 us -> none  [mix_experts(): lax.all_to_all(pair_sum, 'ep', split_axis=0, concat_axis=0, tiled=True)]
    concatenate x4 -> x0, other arithmetic: 3.99 us -> none  [the longest x1 3.16 us: mix_experts(): slot_rows = jnp.concatenate([own_rows, sibling], axis=1)]
  transfers between devices with their start and end apart: 3 -> 0, of which waited for: 3 -> 0; matrix products, arithmetic and copies ran while one was open for 2% -> 0% of each run, Pallas kernels for 0% -> 0%
where the time goes in v1:
time: 49.2 us; the launch traced here: 49 us
  Pallas kernels  44.1 us (90%)
  local copies, waits for them, and re-layouts  4.19 us (9%)
  between operations  0.65 us (1%)
    pallas_call x1, Pallas kernels, shards(): pl.pallas_call(kernel, out_shape=(jax.ShapeDtypeStruct((SEQ_DEV, TILES, L...  44.1 us
    unnamed x4, local copies, waits for them, and re-layouts  4.19 us

profile of v1, /device:TPU:0, one launch (start us, length us, event | category | flops | bytes accessed | tf_op | source)
XLA Modules:
  0.0 49.0 jit_solution(15900507569051595845)
XLA Ops:
  0.6 44.1 %layer.1 = (f32[12,16,128]{2,1,0:T(8,128)}, bf16[12,512]{1,0:T(8,128)(2,1)}, bf16[12,64]{1,0:T(8,128)(2,1)}) custom-call(s32[12]{0:T(128)} %len_s.1, f32[6,12]{1,0:T(8,128)} %bitcast.17, bf16[12,2048]{1,0:T(8,128)(2,1)} %tok.1, f32[1,2048]{1,0:T(1,128)} %bitcast.15, f32[1,512]{1,0:T(1,128)} %bitcast.19, f32[1,512]{1,0:T(1,128)} %bitcast.20, ...), custom_call_target="tpu_custom_call" | custom-call | tf_op jit(solution)/shard_map/layer/pallas_call | solution.py:449
  44.8 0.9 %pad = f32[16,16,128]{2,1,0:T(8,128)S(1)} pad(f32[12,16,128]{2,1,0:T(8,128)} %get-tuple-element.6, f32[]{:T(128)} %constant.12), padding=0_4x0_0x0_0 | pad | bytes 229380
  45.7 0.7 %copy.24 = f32[2,8,16,128]{3,1,2,0:T(8,128)} copy(f32[2,8,16,128]{3,2,1,0:T(8,128)S(1)} %bitcast.12) | data formatting | bytes 262144
  46.4 1.3 %copy.27 = bf16[12,512]{1,0:T(8,128)(2,1)} copy(bf16[12,512]{1,0:T(8,128)(2,1)} %get-tuple-element.13) | data formatting | bytes 24576
  47.7 1.3 %copy.28 = bf16[12,64]{1,0:T(8,128)(2,1)} copy(bf16[12,64]{1,0:T(8,128)(2,1)} %get-tuple-element.14) | data formatting | bytes 3072

commit v2 on v1

--- a/solution.py
+++ b/solution.py
@@ -23,6 +23,9 @@
 SLOTS = CHIPS * CAPACITY
 LANES = 128
 TILES = D // LANES
+FIRST = 9500
+WINDOW = 9000
+GROUP_END = (1, 1, 5, 5, 5, 5, 11, 11, 11, 11, 11, 11)
 PARTS = KV_RANK // LANES
 EPS = 1e-06
 THETA = 10000.0
@@ -47,30 +50,22 @@
     return jnp.concatenate([v[:, half:], v[:, :half]], axis=1)
 
 
-def chip_at(x, y, z):
-    return z * (SIDE * SIDE) + y * SIDE + x
-
-
-def wrap(v):
-    return lax.rem(v + 2 * SIDE, SIDE)
-
-
 def offset_of(p):
-    chunk = p // PER_CHUNK
-    dx = lax.rem(p, SIDE)
-    dy = lax.rem(p // SIDE, SIDE)
-    return dx, dy, wrap(chunk - dx - dy)
+    dx = p % SIDE
+    dy = p // SIDE % SIDE
+    return dx, dy, (p // PER_CHUNK - dx - dy) % SIDE
 
 
 def kernel(
-    len_s, weight_s, tok, ag, qg, kg, mg, ids, inv,
+    len_h, weight_h, tok_h, ag_h, qg_h, kg_h, mg_h, ids_h, inv_h,
     cache, rope_t, qdown, kvdown, krope_t, qup, kup, vup, wout, gate, up, down,
     mixed_o, latent_o, key_o,
+    len_s, weight_s, tok, ag, qg, kg, mg, ids, inv,
     cache_v, rope_v, qdown_v, kvdown_v, krope_v, qup_v, kup_v, vup_v, wout_v,
     gate_v, up_v, down_v,
-    qlat, qrope, scores, olat, own_v, table_v, slot_v, table_s, slot_s,
+    qlat, qrope, olat, own_v, table_v, slot_v, table_s, slot_s,
     tile_f, attn_f, rows_b, send_b, recv_b, out_b, back_b, x_b,
-    w_sem, cache_sem, rope_sem, e_sem, s_sem, x_send, x_recv,
+    i_sem, w_sem, cache_sem, rope_sem, e_sem, s_sem, x_send, x_recv,
     d_send, d_recv, r_send, r_recv,
 ):
     me = lax.axis_index("ep")
@@ -81,52 +76,82 @@
     mz = chip // (SIDE * SIDE)
     sibling = me + 1 - 2 * core
 
-    def target(p, sign):
+    at_x = [lax.rem(mx + i, SIDE) for i in range(SIDE)]
+    at_y = [lax.rem(my + i, SIDE) * SIDE for i in range(SIDE)]
+    at_z = [lax.rem(mz + i, SIDE) * (SIDE * SIDE) for i in range(SIDE)]
+
+    def target(p, sign=1):
         dx, dy, dz = offset_of(p)
-        there = chip_at(wrap(mx + sign * dx), wrap(my + sign * dy), wrap(mz + sign * dz))
-        return there
+        return at_x[sign * dx % SIDE] + at_y[sign * dy % SIDE] + at_z[sign * dz % SIDE]
 
     barrier = pltpu.get_barrier_semaphore()
 
-    weights = [
-        (qdown, qdown_v), (qup, qup_v), (kup, kup_v), (kvdown, kvdown_v), (krope_t, krope_v),
-        (vup, vup_v), (wout, wout_v),
+    sizes = []
+    queue = []
+    began = []
+    done = []
+
+    def later(src, dst, sem, kib):
+        queue.append(pltpu.make_async_copy(src, dst, sem))
+        sizes.append(kib)
+        return len(queue) - 1
+
+    def halves(src, dst, sem, rows, kib):
+        cut = rows // 2
+        for i in range(2):
+            last = later(
+                src.at[i * cut : (i + 1) * cut], dst.at[i * cut : (i + 1) * cut],
+                sem.at[i], kib // 2,
+            )
+        return last
+
+    def cached(t):
+        later(cache.at[t], cache_v.at[t], cache_sem.at[t], 1024)
+        return later(rope_t.at[t], rope_v.at[t], rope_sem.at[t], 128)
+
+    small = [
+        (tok_h, tok), (ag_h, ag), (ids_h, ids), (inv_h, inv), (len_h, len_s),
+        (qg_h, qg), (kg_h, kg), (mg_h, mg), (weight_h, weight_s),
     ]
-    w_copy = [
-        pltpu.make_async_copy(src, dst, w_sem.at[i]) for i, (src, dst) in enumerate(weights)
-    ]
+    small_at = [later(src, dst, i_sem.at[i], 1) for i, (src, dst) in enumerate(small)][-1]
+    qdown_at = halves(qdown, qdown_v, w_sem.at[0], D, 2048)
+    qup_at = halves(qup, qup_v, w_sem.at[1], 512, 1536)
+    kup_at = later(kup, kup_v, w_sem.at[2, 0], 1024)
+    cache_at = [cached(t) for t in range(4)]
+    kvdown_at = halves(kvdown, kvdown_v, w_sem.at[3], D, 2048)
+    krope_at = later(krope_t, krope_v, w_sem.at[4, 0], 256)
+    cache_at += [cached(t) for t in range(4, SEQ_DEV)]
+    vup_at = later(vup, vup_v, w_sem.at[5, 0], 1024)
+    wout_at = halves(wout, wout_v, w_sem.at[6], 1024, 4096)
     experts = [(gate, gate_v), (up, up_v), (down, down_v)]
-    e_copy = [
-        pltpu.make_async_copy(src.at[0], dst.at[0], e_sem.at[i])
-        for i, (src, dst) in enumerate(experts)
-    ]
-
-    def cache_copies(t):
-        return (
-            pltpu.make_async_copy(cache.at[t], cache_v.at[t], cache_sem.at[t]),
-            pltpu.make_async_copy(rope_t.at[t], rope_v.at[t], rope_sem.at[t]),
+    expert_at = [
+        later(src.at[0], dst.at[0], e_sem.at[i], 1024) for i, (src, dst) in enumerate(experts)
+    ][-1]
+
+    def refill(window):
+        while len(began) < len(queue) and (
+            sum(sizes[len(done) : len(began) + 1]) <= window
+        ):
+            queue[len(began)].start(priority=int(len(began) > kup_at))
+            began.append(True)
+
+    def need(last, window=WINDOW):
+        while len(done) <= last:
+            queue[len(done)].wait()
+            done.append(True)
+            refill(window)
+
+    refill(FIRST)
+
+    def signal(sem, device):
+        pl.semaphore_signal(
+            sem, inc=1, device_id=(device,), device_id_type=pl.DeviceIdType.MESH
         )
 
-    def start_cache(t):
-        for c in cache_copies(t):
-            c.start()
-
-    for i in range(5):
-        w_copy[i].start()
-    for t in range(6):
-        start_cache(t)
-
-    def greet(p, carry):
-        pl.semaphore_signal(
-            barrier, inc=1, device_id=(target(p, 1) * 2 + core,),
-            device_id_type=pl.DeviceIdType.MESH,
-        )
-        return carry
-
-    lax.fori_loop(1, CHIPS, greet, 0)
-    pl.semaphore_signal(
-        barrier, inc=1, device_id=(sibling,), device_id_type=pl.DeviceIdType.MESH
-    )
+    for p in range(1, CHIPS):
+        signal(barrier, target(p) * 2 + core)
+    signal(barrier, sibling)
+    need(small_at, FIRST)
 
     ids_v = ids[...]
     table_v[...] = jnp.zeros((8, LANES), jnp.int32)
@@ -177,11 +202,11 @@
     sine = jnp.where(first_half, -sine, sine)[0:SEQ_DEV]
 
     normed = norm_gain(tok[...].astype(F32), ag[...]).astype(BF16)
-    w_copy[0].wait()
+    need(qdown_at)
     q_low = norm_gain(dot(normed, qdown_v[...]), qg[...]).astype(BF16)
-    w_copy[1].wait()
+    need(qup_at)
     query = dot(q_low, qup_v[...])
-    w_copy[2].wait()
+    need(kup_at)
     head_width = NOPE_DIM + ROPE_DIM
     zeros64 = jnp.zeros((SEQ_DEV, LANES - ROPE_DIM), F32)
     for h in range(HEADS):
@@ -192,36 +217,24 @@
         rot = query[:, h * head_width + NOPE_DIM : (h + 1) * head_width]
         rot = rot * cosine + swap_halves(rot) * sine
         qrope[pl.ds(h, SEQ_DEV, stride=HEADS), :] = jnp.concatenate([rot, zeros64], axis=1)
-    w_copy[3].wait()
-    new_latent = norm_gain(dot(normed, kvdown_v[...]), kg[...]).astype(BF16)
-    latent_o[...] = new_latent
-    w_copy[4].wait()
-    new_key = dot_t(normed, krope_v[...])
-    new_key = (new_key * cosine + swap_halves(new_key) * sine).astype(BF16)
-    key_o[...] = new_key
-    own_all = jnp.concatenate([new_latent.astype(F32), new_key.astype(F32), zeros64], axis=1)
-    for t in range(SEQ_DEV):
-        own_v[t] = own_all[t : t + 1, :]
-
     scale = (NOPE_DIM + ROPE_DIM) ** (-0.5)
     position = lax.broadcasted_iota(jnp.int32, (HEADS, CACHE), 1)
 
     def rows_of(t):
-        return pl.ds(pl.multiple_of(t * HEADS, HEADS), HEADS)
+        return slice(t * HEADS, (t + 1) * HEADS)
 
     def query_of(t):
         parts = [qlat[j, rows_of(t), :] for j in range(PARTS)]
         return jnp.concatenate(parts, axis=1).astype(BF16)
 
     def score_step(t):
-        for c in cache_copies(t):
-            c.wait()
+        need(cache_at[GROUP_END[t]])
         q = query_of(t)
         r = qrope[rows_of(t), :].astype(BF16)[:, :ROPE_DIM]
         s = (dot_t(q, cache_v[t]) + dot(r, rope_v[t])) * scale
-        scores[rows_of(t), :] = jnp.where(position < len_s[t], s, -jnp.inf)
-
-    def value_step(t):
+        return jnp.where(position < len_s[t], s, -jnp.inf)
+
+    def value_step(t, s):
         q = query_of(t).astype(F32)
         r = qrope[rows_of(t), :].astype(BF16).astype(F32)
         own_row = own_v[t]
@@ -231,7 +244,6 @@
             jnp.sum(q * own_latent, axis=1, keepdims=True)
             + jnp.sum(r * own_key, axis=1, keepdims=True)
         ) * scale
-        s = scores[rows_of(t), :]
         peak = jnp.maximum(jnp.max(s, axis=1, keepdims=True), own)
         probs = jnp.exp(s - peak)
         own_prob = jnp.exp(own - peak)
@@ -242,60 +254,48 @@
         for j in range(PARTS):
             olat[j, rows_of(t), :] = total[:, j * LANES : (j + 1) * LANES]
 
-    score_step(0)
-    score_step(1)
-
-    def body(i, carry):
-        start_cache(2 * i + 4)
-        start_cache(2 * i + 5)
-        score_step(2 * i)
-        score_step(2 * i + 1)
-        value_step(2 * i - 2)
-        value_step(2 * i - 1)
-        return carry
-
-    lax.fori_loop(1, 3, body, 0)
-    for c in e_copy:
-        c.start()
-    lax.fori_loop(3, 4, body, 0)
-    w_copy[5].start()
-    w_copy[6].start()
-
-    def tail(i, carry):
-        score_step(2 * i)
-        score_step(2 * i + 1)
-        value_step(2 * i - 2)
-        value_step(2 * i - 1)
-        return carry
-
-    lax.fori_loop(4, 5, tail, 0)
-    pl.semaphore_wait(barrier, CHIPS)
-    swap = []
-    for i, (_, dst) in enumerate(experts):
-        e_copy[i].wait()
-        swap.append(
-            pltpu.make_async_remote_copy(
-                src_ref=dst.at[0],
-                dst_ref=dst.at[1],
-                send_sem=x_send.at[i],
-                recv_sem=x_recv.at[i],
-                device_id=(sibling,),
-                device_id_type=pl.DeviceIdType.MESH,
-            )
-        )
-        swap[-1].start()
-    lax.fori_loop(5, 6, tail, 0)
-    value_step(10)
-    value_step(11)
-
-    w_copy[5].wait()
+    held = (score_step(0), score_step(1))
+    need(kvdown_at)
+    new_latent = norm_gain(dot(normed, kvdown_v[...]), kg[...]).astype(BF16)
+    latent_o[...] = new_latent
+    need(krope_at)
+    new_key = dot_t(normed, krope_v[...])
+    new_key = (new_key * cosine + swap_halves(new_key) * sine).astype(BF16)
+    key_o[...] = new_key
+    own_all = jnp.concatenate([new_latent.astype(F32), new_key.astype(F32), zeros64], axis=1)
+    for t in range(SEQ_DEV):
+        own_v[t] = own_all[t : t + 1, :]
+    for i in range(1, SEQ_DEV // 2):
+        fresh = (score_step(2 * i), score_step(2 * i + 1))
+        value_step(2 * i - 2, held[0])
+        value_step(2 * i - 1, held[1])
+        held = fresh
+    value_step(10, held[0])
+    value_step(11, held[1])
+
+    need(vup_at)
     heads = []
     for h in range(HEADS):
         parts = [olat[j, pl.ds(h, SEQ_DEV, stride=HEADS), :] for j in range(PARTS)]
         o = jnp.concatenate(parts, axis=1).astype(BF16)
         heads.append(dot(o, vup_v[:, h * LANES : (h + 1) * LANES]).astype(BF16))
     heads_out = jnp.concatenate(heads, axis=1)
-    w_copy[6].wait()
+    need(wout_at)
+    pl.semaphore_wait(barrier, CHIPS)
+    need(expert_at)
+    swap = [
+        pltpu.make_async_remote_copy(
+            src_ref=dst.at[0],
+            dst_ref=dst.at[1],
+            send_sem=x_send.at[i],
+            recv_sem=x_recv.at[i],
+            device_id=(sibling,),
+            device_id_type=pl.DeviceIdType.MESH,
+        )
+        for i, (_, dst) in enumerate(experts)
+    ]
+    for c in swap:
+        c.start()
     mixed_attn = (tok[...].astype(F32) + dot(heads_out, wout_v[...])).astype(BF16).astype(F32)
     moe_in = norm_gain(mixed_attn, mg[...])
     for j in range(TILES):
@@ -310,17 +310,6 @@
     table_copy.wait()
     slot_copy.wait()
 
-    for s in range(CAPACITY):
-        recv_b[s] = rows_b[table_s[s, chip]]
-
-    def fill(p, carry):
-        there = target(p, 1)
-        for s in range(CAPACITY):
-            send_b[p * CAPACITY + s] = rows_b[table_s[s, there]]
-        return carry
-
-    lax.fori_loop(1, CHIPS, fill, 0)
-
     def block(ref, p, count=1):
         return ref.at[pl.ds(p * CAPACITY, count * CAPACITY)]
 
@@ -344,11 +333,22 @@
             device_id_type=pl.DeviceIdType.MESH,
         )
 
-    def start_dispatch(p, carry):
-        dispatch(p).start()
-        return carry
-
-    lax.fori_loop(1, CHIPS, start_dispatch, 0)
+    def fill(c):
+        for p in range(c * PER_CHUNK, (c + 1) * PER_CHUNK):
+            there = target(p, 1)
+            to = send_b if p else recv_b
+            for s in range(CAPACITY):
+                to[p * CAPACITY + s] = rows_b[table_s[s, there]]
+
+    def send(c):
+        for p in range(max(1, c * PER_CHUNK), (c + 1) * PER_CHUNK):
+            dispatch(p).start()
+
+    fill(0)
+    for c in range(CHUNKS):
+        if c + 1 < CHUNKS:
+            fill(c + 1)
+        send(c)
     for c in swap:
         c.wait()
 
@@ -378,11 +378,8 @@
             back_b[0:CAPACITY] = out[0:CAPACITY]
         out_b[c * ROWS : (c + 1) * ROWS] = out
 
-        def start_back(p, carry):
+        for p in range(c * PER_CHUNK + first, (c + 1) * PER_CHUNK):
             go_back(p).start()
-            return carry
-
-        lax.fori_loop(c * PER_CHUNK + first, (c + 1) * PER_CHUNK, start_back, 0)
 
     for c in range(CHUNKS):
         expert_chunk(c)
@@ -393,10 +390,18 @@
         acc = attn_f[t * TILES : (t + 1) * TILES, :]
         for k in range(TOP_K):
             acc = acc + weight_s[k, t] * back_b[slot_s[k, t]].astype(F32)
-        mixed_o[t] = acc
+        attn_f[t * TILES : (t + 1) * TILES, :] = acc
+    for j in range(TILES):
+        mixed_o[:, j * LANES : (j + 1) * LANES] = attn_f[pl.ds(j, SEQ_DEV, stride=TILES), :]
     sent = block(send_b, 1, CHIPS - 1)
     pltpu.make_async_copy(sent, sent, d_send).wait()
     pltpu.make_async_copy(sent, sent, r_send).wait()
+
+
+def hand_over(mixed, latent, key, mixed_o, latent_o, key_o):
+    mixed_o[...] = mixed[...]
+    latent_o[...] = latent[...]
+    key_o[...] = key[...]
 
 
 def shards(
@@ -408,11 +413,19 @@
     half = ROPE_DIM // 2
     inverse = np.float32(THETA) ** (-np.arange(half, dtype=np.float32) / np.float32(half))
     inverse = jnp.asarray(np.tile(inverse, LANES // half)[None, :].astype(np.float32))
-    smem = pl.BlockSpec(memory_space=pltpu.SMEM)
     vmem = pl.BlockSpec(memory_space=pltpu.VMEM)
     anywhere = pl.BlockSpec(memory_space=pl.ANY)
     dma = pltpu.SemaphoreType.DMA
     scratch = [
+        pltpu.SMEM((SEQ_DEV,), jnp.int32),
+        pltpu.SMEM((TOP_K, SEQ_DEV), F32),
+        pltpu.VMEM((SEQ_DEV, D), BF16),
+        pltpu.VMEM((1, D), F32),
+        pltpu.VMEM((1, 512), F32),
+        pltpu.VMEM((1, KV_RANK), F32),
+        pltpu.VMEM((1, D), F32),
+        pltpu.VMEM((TOP_K, SEQ_DEV), jnp.int32),
+        pltpu.VMEM((1, LANES), F32),
         pltpu.VMEM((SEQ_DEV, CACHE, KV_RANK), BF16),
         pltpu.VMEM((SEQ_DEV, ROPE_DIM, CACHE), BF16),
         pltpu.VMEM((D, 512), BF16),
@@ -427,7 +440,6 @@
         pltpu.VMEM((2, 256, D), BF16),
         pltpu.VMEM((PARTS, SEQ_DEV * HEADS, LANES), F32),
         pltpu.VMEM((SEQ_DEV * HEADS, LANES), F32),
-        pltpu.VMEM((SEQ_DEV * HEADS, CACHE), F32),
         pltpu.VMEM((PARTS, SEQ_DEV * HEADS, LANES), F32),
         pltpu.VMEM((SEQ_DEV, 1, KV_RANK + LANES), F32),
         pltpu.VMEM((8, LANES), jnp.int32),
@@ -442,18 +454,19 @@
         pltpu.VMEM((SLOTS, TILES, LANES), BF16),
         pltpu.VMEM((SLOTS, TILES, LANES), BF16),
         pltpu.VMEM((ROWS, D), BF16),
-        dma((7,)), dma((SEQ_DEV,)), dma((SEQ_DEV,)), dma((3,)), dma((2,)),
+        dma((9,)), dma((7, 2)), dma((SEQ_DEV,)), dma((SEQ_DEV,)), dma((3,)), dma((2,)),
         dma((3,)), dma((3,)),
         dma, dma((CHUNKS,)), dma, dma,
     ]
-    mixed, latent, key = pl.pallas_call(
+    shapes = (
+        jax.ShapeDtypeStruct((SEQ_DEV, D), F32),
+        jax.ShapeDtypeStruct((SEQ_DEV, KV_RANK), BF16),
+        jax.ShapeDtypeStruct((SEQ_DEV, ROPE_DIM), BF16),
+    )
+    done = pl.pallas_call(
         kernel,
-        out_shape=(
-            jax.ShapeDtypeStruct((SEQ_DEV, TILES, LANES), F32),
-            jax.ShapeDtypeStruct((SEQ_DEV, KV_RANK), BF16),
-            jax.ShapeDtypeStruct((SEQ_DEV, ROPE_DIM), BF16),
-        ),
-        in_specs=[smem, smem] + [vmem] * 7 + [anywhere] * 12,
+        out_shape=shapes,
+        in_specs=[anywhere] * 21,
         out_specs=(vmem, vmem, vmem),
         scratch_shapes=scratch,
         compiler_params=pltpu.CompilerParams(
@@ -468,7 +481,13 @@
         w_qdown, w_kvdown, w_krope.T, w_qup, w_kup, w_vup, w_out,
         expert_gate, expert_up, expert_down,
     )
-    return (mixed.reshape(SEQ_DEV, D), latent, key)
+    return pl.pallas_call(
+        hand_over,
+        out_shape=shapes,
+        in_specs=[vmem] * 3,
+        out_specs=(vmem, vmem, vmem),
+        name="outputs",
+    )(*done)
 
 
 def solution(mesh):

time: 49.2 us -> 41.9 us (0.85)
  local copies, waits for them, and re-layouts: 4.19 us -> 0 us
  Pallas kernels: 44.1 us -> 41.1 us
    unnamed x4 -> x0, local copies, waits for them, and re-layouts: 4.19 us -> none
    pallas_call x1 -> x2, Pallas kernels: 44.1 us -> 41.1 us  [the longest x1 39.5 us: shards(): pl.pallas_call(kernel, out_shape=shapes, in_specs=[anywhere] * 21, out_sp...]
where the time goes in v2:
time: 41.9 us; the launch traced here: 41.8 us
  Pallas kernels  41.1 us (98%)
  between operations  0.65 us (2%)
    pallas_call x1, Pallas kernels, shards(): pl.pallas_call(kernel, out_shape=shapes, in_specs=[anywhere] * 21, out_sp...  39.5 us
    pallas_call x1, Pallas kernels, shards(): pl.pallas_call(hand_over, out_shape=shapes, in_specs=[vmem] * 3, out_spec...  1.59 us

profile of v2, /device:TPU:0, one launch (start us, length us, event | category | flops | bytes accessed | tf_op | source)
XLA Modules:
  0.0 41.8 jit_solution(7154142688040842209)
XLA Ops:
  0.6 39.5 %layer.1 = (f32[12,2048]{1,0:T(8,128)}, bf16[12,512]{1,0:T(8,128)(2,1)}, bf16[12,64]{1,0:T(8,128)(2,1)}) custom-call(s32[12]{0:T(128)} %len_h.1, f32[6,12]{1,0:T(8,128)} %bitcast.12, bf16[12,2048]{1,0:T(8,128)(2,1)} %tok_h.1, f32[1,2048]{1,0:T(1,128)} %bitcast.10, f32[1,512]{1,0:T(1,128)} %bitcast.14, f32[1,512]{1,0:T(1,128)} %bitcast.15, ...), custom_call_target="tpu_custom_call" | custom-call | tf_op jit(solution)/shard_map/layer/pallas_call | solution.py:466
  40.2 1.6 %outputs.1 = (f32[12,2048]{1,0:T(8,128)}, bf16[12,512]{1,0:T(8,128)(2,1)}, bf16[12,64]{1,0:T(8,128)(2,1)}) custom-call(f32[12,2048]{1,0:T(8,128)} %get-tuple-element.6.mixed, bf16[12,512]{1,0:T(8,128)(2,1)} %get-tuple-element.7.latent, bf16[12,64]{1,0:T(8,128)(2,1)} %get-tuple-element.8.key), custom_call_target="tpu_custom_call" | custom-call | tf_op jit(solution)/shard_map/outputs/pallas_call | solution.py:484

commit v3 on v2

--- a/solution.py
+++ b/solution.py
@@ -53,7 +53,7 @@
 def offset_of(p):
     dx = p % SIDE
     dy = p // SIDE % SIDE
-    return dx, dy, (p // PER_CHUNK - dx - dy) % SIDE
+    return dx, dy, (p // (SIDE * SIDE) - dx - dy) % SIDE
 
 
 def kernel(
@@ -182,7 +182,7 @@
         dx = ((e & 3) - mx) & 3
         dy = (((e >> 2) & 3) - my) & 3
         dz = ((e >> 4) - mz) & 3
-        place = ((dx + dy + dz) & 3) * PER_CHUNK + dx + SIDE * dy
+        place = ((dx + dy + dz) & 3) * (SIDE * SIDE) + dx + SIDE * dy
         slot_v[k : k + 1, 0:SEQ_DEV] = place * CAPACITY + jnp.clip(
             own_rank.astype(jnp.int32), 0, CAPACITY - 1
         )
@@ -396,12 +396,6 @@
     sent = block(send_b, 1, CHIPS - 1)
     pltpu.make_async_copy(sent, sent, d_send).wait()
     pltpu.make_async_copy(sent, sent, r_send).wait()
-
-
-def hand_over(mixed, latent, key, mixed_o, latent_o, key_o):
-    mixed_o[...] = mixed[...]
-    latent_o[...] = latent[...]
-    key_o[...] = key[...]
 
 
 def shards(
@@ -458,14 +452,13 @@
         dma((3,)), dma((3,)),
         dma, dma((CHUNKS,)), dma, dma,
     ]
-    shapes = (
-        jax.ShapeDtypeStruct((SEQ_DEV, D), F32),
-        jax.ShapeDtypeStruct((SEQ_DEV, KV_RANK), BF16),
-        jax.ShapeDtypeStruct((SEQ_DEV, ROPE_DIM), BF16),
-    )
-    done = pl.pallas_call(
+    return pl.pallas_call(
         kernel,
-        out_shape=shapes,
+        out_shape=(
+            pltpu.VMEM((SEQ_DEV, D), F32),
+            pltpu.VMEM((SEQ_DEV, KV_RANK), BF16),
+            pltpu.VMEM((SEQ_DEV, ROPE_DIM), BF16),
+        ),
         in_specs=[anywhere] * 21,
         out_specs=(vmem, vmem, vmem),
         scratch_shapes=scratch,
@@ -481,13 +474,6 @@
         w_qdown, w_kvdown, w_krope.T, w_qup, w_kup, w_vup, w_out,
         expert_gate, expert_up, expert_down,
     )
-    return pl.pallas_call(
-        hand_over,
-        out_shape=shapes,
-        in_specs=[vmem] * 3,
-        out_specs=(vmem, vmem, vmem),
-        name="outputs",
-    )(*done)
 
 
 def solution(mesh):

time: 41.9 us -> 41.5 us (level)
  Pallas kernels: 41.1 us -> 38.9 us
  local copies, waits for them, and re-layouts: 0 us -> 1.85 us
    pallas_call x2 -> x1, Pallas kernels: 41.1 us -> 38.9 us  [shards(): pl.pallas_call(kernel, out_shape=(pltpu.VMEM((SEQ_DEV, D), F32), pltpu.VM...]
    unnamed x0 -> x3, local copies, waits for them, and re-layouts: none -> 1.85 us
where the time goes in v3:
time: 41.5 us; the launch traced here: 41.4 us
  Pallas kernels  38.9 us (94%)
  local copies, waits for them, and re-layouts  1.85 us (4%)
  between operations  0.65 us (2%)
    pallas_call x1, Pallas kernels, shards(): pl.pallas_call(kernel, out_shape=(pltpu.VMEM((SEQ_DEV, D), F32), pltpu.VM...  38.9 us
    unnamed x3, local copies, waits for them, and re-layouts  1.85 us

profile of v3, /device:TPU:0, one launch (start us, length us, event | category | flops | bytes accessed | tf_op | source)
XLA Modules:
  0.0 41.4 jit_solution(1743541370005019336)
XLA Ops:
  0.6 38.9 %layer.1 = (f32[12,2048]{1,0:T(8,128)S(1)}, bf16[12,512]{1,0:T(8,128)(2,1)S(1)}, bf16[12,64]{1,0:T(8,128)(2,1)S(1)}) custom-call(s32[12]{0:T(128)} %len_h.1, f32[6,12]{1,0:T(8,128)} %bitcast.12, bf16[12,2048]{1,0:T(8,128)(2,1)} %tok_h.1, f32[1,2048]{1,0:T(1,128)} %bitcast.10, f32[1,512]{1,0:T(1,128)} %bitcast.14, f32[1,512]{1,0:T(1,128)} %bitcast.15, ...), custom_call_target="tpu_custom_call" | custom-call | tf_op jit(solution)/shard_map/layer/pallas_call | solution.py:455
  39.5 0.7 %copy.27 = f32[12,2048]{1,0:T(8,128)} copy(f32[12,2048]{1,0:T(8,128)S(1)} %get-tuple-element.3) | data formatting | bytes 196608
  40.2 0.6 %copy.29 = bf16[12,64]{1,0:T(8,128)(2,1)} copy(bf16[12,64]{1,0:T(8,128)(2,1)S(1)} %get-tuple-element.5) | data formatting | bytes 3072
  40.8 0.6 %copy.28 = bf16[12,512]{1,0:T(8,128)(2,1)} copy(bf16[12,512]{1,0:T(8,128)(2,1)S(1)} %get-tuple-element.4) | data formatting | bytes 24576

commit v4 on v3

--- a/solution.py
+++ b/solution.py
@@ -432,16 +432,16 @@
         pltpu.VMEM((2, D, 256), BF16),
         pltpu.VMEM((2, D, 256), BF16),
         pltpu.VMEM((2, 256, D), BF16),
-        pltpu.VMEM((PARTS, SEQ_DEV * HEADS, LANES), F32),
-        pltpu.VMEM((SEQ_DEV * HEADS, LANES), F32),
-        pltpu.VMEM((PARTS, SEQ_DEV * HEADS, LANES), F32),
-        pltpu.VMEM((SEQ_DEV, 1, KV_RANK + LANES), F32),
+        pltpu.VMEM((PARTS, 16 * HEADS, LANES), F32),
+        pltpu.VMEM((16 * HEADS, LANES), F32),
+        pltpu.VMEM((PARTS, 16 * HEADS, LANES), F32),
+        pltpu.VMEM((SEQ_DEV + 8, 1, KV_RANK + LANES), F32),
         pltpu.VMEM((8, LANES), jnp.int32),
         pltpu.VMEM((8, LANES), jnp.int32),
         pltpu.SMEM((8, LANES), jnp.int32),
         pltpu.SMEM((8, LANES), jnp.int32),
         pltpu.VMEM((ROWS * TILES, LANES), F32),
-        pltpu.VMEM((SEQ_DEV * TILES, LANES), F32),
+        pltpu.VMEM((16 * TILES, LANES), F32),
         pltpu.VMEM((SEQ_DEV + 1, TILES, LANES), BF16),
         pltpu.VMEM((SLOTS, TILES, LANES), BF16),
         pltpu.VMEM((SLOTS, TILES, LANES), BF16),

time: 41.5 us -> 41.5 us (level)
  no operation moved by 1% of the time
where the time goes in v4:
time: 41.5 us; the launch traced here: 41.4 us
  Pallas kernels  38.9 us (94%)
  local copies, waits for them, and re-layouts  1.85 us (4%)
  between operations  0.65 us (2%)
    pallas_call x1, Pallas kernels, shards(): pl.pallas_call(kernel, out_shape=(pltpu.VMEM((SEQ_DEV, D), F32), pltpu.VM...  38.9 us
    unnamed x3, local copies, waits for them, and re-layouts  1.85 us

profile of v4, /device:TPU:0, one launch (start us, length us, event | category | flops | bytes accessed | tf_op | source)
XLA Modules:
  0.0 41.4 jit_solution(1293526076798495449)
XLA Ops:
  0.6 38.9 %layer.1 = (f32[12,2048]{1,0:T(8,128)S(1)}, bf16[12,512]{1,0:T(8,128)(2,1)S(1)}, bf16[12,64]{1,0:T(8,128)(2,1)S(1)}) custom-call(s32[12]{0:T(128)} %len_h.1, f32[6,12]{1,0:T(8,128)} %bitcast.12, bf16[12,2048]{1,0:T(8,128)(2,1)} %tok_h.1, f32[1,2048]{1,0:T(1,128)} %bitcast.10, f32[1,512]{1,0:T(1,128)} %bitcast.14, f32[1,512]{1,0:T(1,128)} %bitcast.15, ...), custom_call_target="tpu_custom_call" | custom-call | tf_op jit(solution)/shard_map/layer/pallas_call | solution.py:455
  39.5 0.7 %copy.27 = f32[12,2048]{1,0:T(8,128)} copy(f32[12,2048]{1,0:T(8,128)S(1)} %get-tuple-element.3) | data formatting | bytes 196608
  40.2 0.6 %copy.29 = bf16[12,64]{1,0:T(8,128)(2,1)} copy(bf16[12,64]{1,0:T(8,128)(2,1)S(1)} %get-tuple-element.5) | data formatting | bytes 3072
  40.8 0.6 %copy.28 = bf16[12,512]{1,0:T(8,128)(2,1)} copy(bf16[12,512]{1,0:T(8,128)(2,1)S(1)} %get-tuple-element.4) | data formatting | bytes 24576
